TPU v7x, 32 devices: a whole 2x2x4 slice. The times are simulated.
32 devices in a mesh: fs: 8 (over z, x), tp: 4 (over y, core).
Axes of the slice: x: 2, y: 2, z: 4, core: 2. Of those that a mesh axis runs over, the one named last changes fastest.
Arguments:
- inputs: bfloat16 [2048, 2048], P('fs'), may hold values from -6 to 6
- cotangent: bfloat16 [2048, 2048], P('fs'), may hold values from -8 to 8
- up_weight: float32 [2048, 2944], P('fs', 'tp'), may hold values from -0.125 to 0.125
- gate_weight: float32 [2048, 2944], P('fs', 'tp'), may hold values from -0.125 to 0.125
- down_weight: float32 [2944, 2048], P('tp', 'fs'), may hold values from -0.109375 to 0.109375
- up_scale: float32 [2944], P('tp'), may hold values from 0.5 to 2
- gate_scale: float32 [2944], P('tp'), may hold values from 0.5 to 2
- down_scale: float32 [2048], replicated, may hold values from 0.5 to 2
- conv_weight: float32 [3, 2944], P(None, 'tp'), may hold values from -3.5 to 3.5
- conv_bias: float32 [2944], P('tp'), may hold values from -3 to 3
Outputs:
- grad_input: bfloat16 [2048, 2048], P('fs')
- grad_up: float32 [2048, 2944], P('fs', 'tp')
- grad_gate: float32 [2048, 2944], P('fs', 'tp')
- grad_down: float32 [2944, 2048], P('tp', 'fs')
- grad_conv: float32 [3, 2944], P(None, 'tp')
- grad_bias: float32 [2944], P('tp')
All inputs are finite; a program needn't handle non-finite values.
Results may differ from a plain program's by a relative error of at most 0.018.
Values may be sent and summed in bfloat16 or wider, within the bound.
No kernel may reach another device: no remote copies, remote signals or barrier semaphores. Data moves between devices by JAX's collectives and lax.ppermute only.
A program may use at most 64 MiB of HBM per device.

v0:
```python
import jax
import jax.numpy as jnp
from jax import lax
from jax.sharding import PartitionSpec as P

TAPS = 3


def causal_conv(act, conv_weight, conv_bias):
    length = act.shape[0]
    padded = jnp.pad(act, ((TAPS - 1, 0), (0, 0)))
    result = conv_bias + jnp.zeros_like(act)
    for offset in range(TAPS):
        result = result + padded[offset : offset + length] * conv_weight[offset]
    return (result, padded)


def conv_back(conv_cot, padded, conv_weight):
    length = conv_cot.shape[0]
    padded_cot = jnp.pad(conv_cot, ((0, TAPS - 1), (0, 0)))
    act_cot = jnp.zeros_like(conv_cot)
    tap_grads = []
    for offset in range(TAPS):
        shift_start = TAPS - 1 - offset
        act_cot = act_cot + conv_weight[offset] * padded_cot[shift_start : shift_start + length]
        tap_grads.append(jnp.sum(conv_cot * padded[offset : offset + length], axis=0))
    return (act_cot, jnp.stack(tap_grads), jnp.sum(conv_cot, axis=0))


def contract_last(left, right):
    return lax.dot_general(
        left, right, (((1,), (1,)), ((), ())), preferred_element_type=jnp.float32
    )


def contract_first(left, right):
    return lax.dot_general(
        left, right, (((0,), (0,)), ((), ())), preferred_element_type=jnp.float32
    )


def on_device(
    inputs,
    cotangent,
    up_weight,
    gate_weight,
    down_weight,
    up_scale,
    gate_scale,
    down_scale,
    conv_weight,
    conv_bias,
):
    pair_half = jnp.stack([up_weight.astype(jnp.bfloat16), gate_weight.astype(jnp.bfloat16)])
    down_half = down_weight.astype(jnp.bfloat16)
    full_pair = lax.all_gather(pair_half, "fs", axis=1, tiled=True)
    up_act = jnp.dot(inputs, full_pair[0], preferred_element_type=jnp.float32) * up_scale
    gate_act = jnp.dot(inputs, full_pair[1], preferred_element_type=jnp.float32) * gate_scale
    conv_out, padded = causal_conv(up_act, conv_weight, conv_bias)
    gelu_val, gelu_back = jax.vjp(jax.nn.gelu, conv_out)
    hidden = (gelu_val * gate_act).astype(jnp.bfloat16)
    full_down = lax.all_gather(down_half, "fs", axis=1, tiled=True)
    scaled_cot = (cotangent.astype(jnp.float32) * down_scale).astype(jnp.bfloat16)
    hidden_cot = contract_last(scaled_cot, full_down)
    gate_cot = (hidden_cot * gelu_val * gate_scale).astype(jnp.bfloat16)
    (conv_cot,) = gelu_back(hidden_cot * gate_act)
    act_cot, tap_part, bias_part = conv_back(conv_cot, padded, conv_weight)
    up_cot = (act_cot * up_scale).astype(jnp.bfloat16)
    grad_conv, grad_bias = lax.psum((tap_part, bias_part), "fs")
    partial_sum = contract_last(up_cot, full_pair[0]) + contract_last(gate_cot, full_pair[1])
    grad_input = lax.psum(partial_sum.astype(jnp.bfloat16), "tp")
    up_term = contract_first(inputs, up_cot)
    gate_term = contract_first(inputs, gate_cot)
    down_part = lax.psum_scatter(
        contract_first(scaled_cot, hidden).astype(jnp.bfloat16),
        "fs",
        scatter_dimension=0,
        tiled=True,
    ).astype(jnp.float32)
    up_pieces, gate_pieces = (
        lax.all_to_all(
            up_term[None].astype(jnp.bfloat16), "fs", split_axis=1, concat_axis=0, tiled=True
        ).astype(jnp.float32),
        lax.all_to_all(
            gate_term[None].astype(jnp.bfloat16), "fs", split_axis=1, concat_axis=0, tiled=True
        ).astype(jnp.float32),
    )
    grad_up = jnp.sum(up_pieces, axis=0)
    grad_gate = jnp.sum(gate_pieces, axis=0)
    grad_down = down_part.T
    return (grad_input, grad_up, grad_gate, grad_down, grad_conv, grad_bias)


def solution(mesh):
    in_specs = (
        P("fs", None),
        P("fs", None),
        P("fs", "tp"),
        P("fs", "tp"),
        P("tp", "fs"),
        P("tp"),
        P("tp"),
        P(),
        P(None, "tp"),
        P("tp"),
    )
    out_specs = (P("fs", None), P("fs", "tp"), P("fs", "tp"), P("tp", "fs"), P(None, "tp"), P("tp"))
    return jax.shard_map(
        on_device, mesh=mesh, in_specs=in_specs, out_specs=out_specs, check_vma=False
    )
```

profile of v0, /device:TPU:0, one launch (start us, length us, event | category | flops | bytes accessed | tf_op | source)
XLA Modules:
  0.0 520.8 jit_solution(11268263426543654866)
XLA Ops:
  7.2 0.0 copy-start
  7.2 0.0 all-gather.5.cloned.1.call-start
  7.3 1.5 convert_bitcast_fusion.1
  8.8 0.9 pad_maximum_fusion
  9.7 0.0 all-gather.5.cloned.1.call-update
  9.8 0.0 all-gather.3.cloned.1.call-start
  9.8 0.8 convert_element_type.73
  10.6 0.0 all-gather.3.cloned.1.call-update
  10.7 99.0 %all-gather.5.cloned.1.call-done = bf16[2,2048,736]{1,2,0:T(8,128)(2,1)} async-done(((bf16[2,256,736]{1,2,0:T(8,128)(2,1)}), bf16[2,2048,736]{1,2,0:T(8,128)(2,1)}) %all-gather.5.cloned.1.call-update) | async-done | bytes 6029328 | tf_op jit(solution)/shard_map/all_gather | solution.py:56
  109.7 3.9 fusion.9
  113.6 1.9 fusion.7
  115.4 56.2 %all-gather.3.cloned.1.call-done = bf16[736,2048]{1,0:T(8,128)(2,1)} async-done(((bf16[736,256]{1,0:T(8,128)(2,1)}), bf16[736,2048]{1,0:T(8,128)(2,1)}) %all-gather.3.cloned.1.call-update) | async-done | bytes 3014672 | tf_op jit(solution)/shard_map/all_gather | solution.py:62
  171.7 6.2 %multiply_reduce_fusion.2 = (f32[736]{0:T(1024)S(1)}, f32[736]{0:T(1024)S(1)}, f32[736]{0:T(1024)S(1)}, f32[736]{0:T(1024)S(1)}, f32[256,736]{0,1:T(8,128)}, /*index=5*/f32[256,736]{0,1:T(8,128)S(1)}, f32[256,736]{0,1:T(8,128)S(1)}) fusion(f32[256,736]{0,1:T(8,128)} %fusion.7, f32[256,736]{0,1:T(8,128)} %fusion.9, f32[736]{0:T(1024)S(1)} %get-tuple-element.11, ...), kind=kOutput, calls=%fused_computation.42 | convolution fusion | flops 779539456 | bytes 7863296 | tf_op jit(solution)/shard_map/dot_general | solution.py:31
  177.9 0.3 multiply_convert_fusion.4
  178.1 2.6 fusion.1
  180.7 15.8 %copy.24 = bf16[1,2048,736]{2,0,1:T(2,128)(2,1)} copy(bf16[1,2048,736]{1,2,0:T(8,128)(2,1)} %fusion.1) | data formatting | bytes 6029312 | tf_op jit(solution)/shard_map/convert_element_type | solution.py:85
  196.5 0.5 broadcast.62
  197.0 36.3 %reduce.7 = bf16[2048,736]{1,0:T(8,128)(2,1)} reduce(bf16[2048,1,736]{2,1,0:T(2,128)(2,1)} %bitcast.61, bf16[]{:T(256)} %broadcast.62), dimensions={1}, to_apply=%bitcast.50.reduce_sub_computation | reduce | bytes 6029314
  233.3 8.4 %reshape.35 = bf16[8,2,94208]{2,1,0:T(2,128)(2,1)} reshape(bf16[2048,736]{1,0:T(8,128)(2,1)} %reduce.7) | data formatting | bytes 6029312
  241.7 4.4 all-to-all-start.1
  246.1 0.2 reduce-scatter.2.cloned.1.call-start
  246.4 3.9 convolution_convert_fusion
  250.2 0.0 reduce-scatter.2.cloned.1.call-update
  250.3 1.1 copy-done.5
  251.3 0.8 fusion.21
  252.2 2.6 fusion
  254.8 15.7 %copy.22 = bf16[1,2048,736]{2,0,1:T(2,128)(2,1)} copy(bf16[1,2048,736]{1,2,0:T(8,128)(2,1)} %fusion) | data formatting | bytes 6029312 | tf_op jit(solution)/shard_map/convert_element_type | solution.py:82
  270.5 36.3 %reduce.6 = bf16[2048,736]{1,0:T(8,128)(2,1)} reduce(bf16[2048,1,736]{2,1,0:T(2,128)(2,1)} %bitcast.62, bf16[]{:T(256)} %broadcast.62), dimensions={1}, to_apply=%bitcast.48.reduce_sub_computation | reduce | bytes 6029314
  306.8 8.4 %reshape.33 = bf16[8,2,94208]{2,1,0:T(2,128)(2,1)} reshape(bf16[2048,736]{1,0:T(8,128)(2,1)} %reduce.6) | data formatting | bytes 6029312
  315.2 22.6 %all-to-all-done.1 = bf16[8,2,94208]{2,1,0:T(2,128)(2,1)} async-done(((bf16[8,2,94208]{2,1,0:T(2,128)(2,1)}), bf16[8,2,94208]{2,1,0:T(2,128)(2,1)}, u32[]{:S(2)}, u32[]{:S(2)}) %all-to-all-start.1) | async-done | bytes 3014688 | tf_op jit(solution)/shard_map/all_to_all | solution.py:84
  337.8 4.4 all-to-all-start
  342.3 0.0 all-reduce.5.cloned.1.call-start
  342.4 2.9 fusion.3
  345.2 3.9 fusion.5
  349.1 0.0 all-reduce.5.cloned.1.call-update
  349.1 96.4 %all-reduce.2 = (f32[3,736]{1,0:T(4,128)}, f32[736]{0:T(1024)}) all-reduce(f32[3,736]{1,0:T(4,128)S(1)} %pad_maximum_fusion.1, f32[736]{0:T(1024)S(1)} %get-tuple-element.9), channel_id=1, replica_groups=mesh['fs'=8,'tp'=4] {'fs'}, use_global_device_ids=true, to_apply=%region_7.8 | all-reduce | flops 2944 | bytes 23552 | tf_op jit(solution)/shard_map/psum | solution.py:69
  445.5 8.8 %reshape.36 = bf16[2048,1,736]{2,1,0:T(2,128)(2,1)} reshape(bf16[8,2,94208]{2,1,0:T(2,128)(2,1)} %all-to-all-done.1) | data formatting | bytes 6029312
  454.2 15.3 %copy.25 = bf16[1,2048,736]{1,2,0:T(8,128)(2,1)} copy(bf16[1,2048,736]{2,0,1:T(2,128)(2,1)} %bitcast.63) | data formatting | bytes 6029312 | tf_op jit(solution)/shard_map/all_to_all | solution.py:84
  469.5 2.6 convert_element_type.92
  472.2 2.9 copy.27
  475.1 2.7 bitcast_reduce_fusion
  477.8 8.8 %reshape.34 = bf16[2048,1,736]{2,1,0:T(2,128)(2,1)} reshape(bf16[8,2,94208]{2,1,0:T(2,128)(2,1)} %all-to-all-done) | data formatting | bytes 6029312
  486.5 15.3 %copy.23 = bf16[1,2048,736]{1,2,0:T(8,128)(2,1)} copy(bf16[1,2048,736]{2,0,1:T(2,128)(2,1)} %bitcast.64) | data formatting | bytes 6029312 | tf_op jit(solution)/shard_map/all_to_all | solution.py:81
  501.8 2.6 convert_element_type.91
  504.5 2.9 copy.26
  507.4 2.7 bitcast_reduce_fusion.1
  510.1 1.9 convert_bitcast_fusion
  512.0 2.3 copy.29
  (28 shorter events, 0.1 us)
Async XLA Ops:
  7.2 102.5 %copy-start = (bf16[256,2048]{1,0:T(8,128)(2,1)S(1)}, bf16[256,2048]{1,0:T(8,128)(2,1)}, u32[]{:S(2)}) copy-start(bf16[256,2048]{1,0:T(8,128)(2,1)} %param.10) | copy-start | bytes 3145732
  7.2 2.6 copy-start.4
  7.2 3.4 copy-start.7
  7.2 102.5 %copy-start.8 = (f32[736]{0:T(1024)S(1)}, f32[736]{0:T(1024)}, u32[]{:S(2)}) copy-start(f32[736]{0:T(1024)} %param.16) | copy-start | bytes 8836
  7.2 102.5 %all-gather.5.cloned.1.call-start = ((), (), s32[]{:S(2)}) async-start(), calls=%async_computation.4 | async-start | bytes 6782976 | tf_op jit(solution)/shard_map/all_gather | solution.py:56
  9.8 161.9 %all-gather.3.cloned.1.call-start = ((), (), s32[]{:S(2)}) async-start(), calls=%async_computation.3 | async-start | bytes 3391488 | tf_op jit(solution)/shard_map/all_gather | solution.py:62
  10.7 102.9 %copy-start.9 = (f32[736]{0:T(1024)S(1)}, f32[736]{0:T(1024)}, u32[]{:S(2)}) copy-start(f32[736]{0:T(1024)} %param.15) | copy-start | bytes 8836
  109.7 3.9 copy-start.2
  113.6 58.1 %copy-start.3 = (bf16[256,2048]{1,0:T(8,128)(2,1)S(1)}, bf16[256,2048]{1,0:T(8,128)(2,1)}, u32[]{:S(2)}) copy-start(bf16[256,2048]{1,0:T(8,128)(2,1)} %param.11) | copy-start | bytes 3145732
  113.6 58.1 %copy-start.6 = (f32[2048]{0:T(1024)S(1)}, f32[2048]{0:T(1024)}, u32[]{:S(2)}) copy-start(f32[2048]{0:T(1024)} %param.17) | copy-start | bytes 24580
  113.6 58.1 %copy-start.10 = (f32[736]{0:T(1024)S(1)}, f32[736]{0:T(1024)}, u32[]{:S(2)}) copy-start(f32[736]{0:T(1024)} %param.19) | copy-start | bytes 8836
  241.7 96.1 %all-to-all-start.1 = ((bf16[8,2,94208]{2,1,0:T(2,128)(2,1)}), bf16[8,2,94208]{2,1,0:T(2,128)(2,1)}, u32[]{:S(2)}, u32[]{:S(2)}) async-start(bf16[8,2,94208]{2,1,0:T(2,128)(2,1)} %reshape.35), calls=%async_computation.1 | async-start | bytes 6029312 | tf_op jit(solution)/shard_map/all_to_all | solution.py:84
  246.1 263.9 %reduce-scatter.2.cloned.1.call-start = ((), (), s32[]{:S(2)}) async-start(), calls=%async_computation.6 | async-start | bytes 3391488 | tf_op jit(solution)/shard_map/reduce_scatter | solution.py:74
  250.2 1.1 copy-start.5
  337.8 140.0 %all-to-all-start = ((bf16[8,2,94208]{2,1,0:T(2,128)(2,1)}), bf16[8,2,94208]{2,1,0:T(2,128)(2,1)}, u32[]{:S(2)}, u32[]{:S(2)}) async-start(bf16[8,2,94208]{2,1,0:T(2,128)(2,1)} %reshape.33), calls=%async_computation | async-start | bytes 6029312 | tf_op jit(solution)/shard_map/all_to_all | solution.py:81
  342.3 169.7 %all-reduce.5.cloned.1.call-start = ((), (), s32[]{:S(2)}) async-start(), calls=%async_computation.5 | async-start | bytes 2097152 | tf_op jit(solution)/shard_map/psum | solution.py:71
  507.4 6.9 %copy-start.1 = (bf16[256,2048]{1,0:T(8,128)(2,1)S(1)}, bf16[256,2048]{1,0:T(8,128)(2,1)}, u32[]{:S(2)}) copy-start(bf16[256,2048]{1,0:T(8,128)(2,1)} %param.10) | copy-start | bytes 3145732
Sparse Core Ops, SparseCore 0:
  10.6 99.0 all-gather.4
  112.3 59.3 all-gather.2
  250.5 130.0 reduce-scatter.1
  383.4 61.8 all-reduce.4
where the time goes:
time: 524 us; the launch traced here: 521 us
  waiting for transfers between devices  178 us (34%)
  local copies, waits for them, and re-layouts  106 us (20%)
  blocking collectives  96.4 us (18%)
  other arithmetic  89.6 us (17%)
  matrix products  27.6 us (5%)
  between operations  14 us (3%)
  starting transfers between devices  9.21 us (2%)
    all_gather x1, waiting for transfers between devices, on_device(): full_pair = lax.all_gather(pair_half, 'fs', axis=1, tiled=True)  99 us
    psum x1, blocking collectives, on_device(): grad_conv, grad_bias = lax.psum((tap_part, bias_part), 'fs')  96.4 us
    unnamed x2, other arithmetic  72.6 us
    all_gather x1, waiting for transfers between devices, on_device(): full_down = lax.all_gather(down_half, 'fs', axis=1, tiled=True)  56.2 us
    unnamed x30, local copies, waits for them, and re-layouts  44.1 us
    all_to_all x1, waiting for transfers between devices, on_device(): lax.all_to_all(gate_term[None].astype(jnp.bfloat16), 'fs', split_axis=1,...  22.6 us
    convert_element_type x1, local copies, waits for them, and re-layouts, on_device(): gate_term[None].astype(jnp.bfloat16)  15.8 us
    convert_element_type x1, local copies, waits for them, and re-layouts, on_device(): up_term[None].astype(jnp.bfloat16)  15.7 us
  transfers between devices with their start and end apart: 6, of which 3 were waited for; matrix products, arithmetic and copies ran while one was open for 28% of the time, Pallas kernels for 0%

commit v1 on v0

v1 whole, which is shorter than its diff:
```python
import jax
import jax.numpy as jnp
from jax import lax
from jax.sharding import Mesh
from jax.sharding import PartitionSpec as P

TAPS = 3


def dot_f32(left, right, left_dim, right_dim):
    return lax.dot_general(
        left, right, (((left_dim,), (right_dim,)), ((), ())), preferred_element_type=jnp.float32
    )


def swap(value):
    return lax.ppermute(value, "fx", [(0, 1), (1, 0)])


def column(vector):
    return vector[:, None]


def later(act, step, position):
    if step == 0:
        return act
    moved = jnp.pad(act, ((0, 0), (step, 0)))[:, : act.shape[1]]
    return jnp.where(position >= step, moved, 0.0)


def earlier(act, step, position, length):
    if step == 0:
        return act
    moved = jnp.pad(act, ((0, 0), (0, step)))[:, step:]
    return jnp.where(position < length - step, moved, 0.0)


def sum_over_fz(value, n_fz):
    if n_fz & (n_fz - 1):
        return lax.psum(value, "fz")
    step = 1
    while step < n_fz:
        value = value + lax.ppermute(value, "fz", [(i, i ^ step) for i in range(n_fz)])
        step *= 2
    return value


def sum_over_tp(partial, n_tp):
    rows = partial.shape[0] // n_tp
    me = lax.axis_index("tp")

    def piece(index):
        return lax.dynamic_slice_in_dim(partial, index * rows, rows, 0)

    total = piece(me).astype(jnp.float32)
    for shift in range(1, n_tp):
        ring = [(i, (i + shift) % n_tp) for i in range(n_tp)]
        got = lax.ppermute(piece((me + shift) % n_tp), "tp", ring)
        total = total + got.astype(jnp.float32)
    own = total.astype(jnp.bfloat16)
    result = lax.dynamic_update_slice_in_dim(jnp.zeros_like(partial), own, me * rows, 0)
    for shift in range(1, n_tp):
        ring = [(i, (i + shift) % n_tp) for i in range(n_tp)]
        got = lax.ppermute(own, "tp", ring)
        source = (me - shift) % n_tp
        result = lax.dynamic_update_slice_in_dim(result, got, source * rows, 0)
    return result


def make_on_device(n_fz, n_tp):
    def on_device(
        inputs,
        cotangent,
        up_weight,
        gate_weight,
        down_weight,
        up_scale,
        gate_scale,
        down_scale,
        conv_weight,
        conv_bias,
    ):
        bf16 = jnp.bfloat16
        low = lax.axis_index("fx") == 0
        length = inputs.shape[0]
        half = down_weight.shape[0] // 2
        width = down_weight.shape[1]

        def mine(value, axis=0):
            first, second = jnp.split(value, 2, axis=axis)
            return jnp.where(low, first, second)

        def theirs(value, axis=0):
            first, second = jnp.split(value, 2, axis=axis)
            return jnp.where(low, second, first)

        def in_order(own, other, axis):
            return jnp.concatenate(
                [jnp.where(low, own, other), jnp.where(low, other, own)], axis=axis
            )

        def gather(weights):
            stored = jnp.stack([w.astype(bf16) for w in weights])
            block = in_order(mine(stored, 1), swap(theirs(stored, 1)), 2)
            return lax.all_gather(block, "fz", axis=2, tiled=True)

        full_pair = gather([up_weight.T, gate_weight.T])
        full_down = gather([down_weight])[0]
        tokens = jnp.concatenate([inputs, swap(inputs)], axis=0)
        scaled_own = (cotangent.astype(jnp.float32) * down_scale).astype(bf16)
        scaled_cot = jnp.concatenate([scaled_own, swap(scaled_own)], axis=0)
        up_col = column(mine(up_scale))
        gate_col = column(mine(gate_scale))
        taps = mine(conv_weight, 1)
        bias_col = column(mine(conv_bias))
        position = lax.broadcasted_iota(jnp.int32, (1, 2 * length), 1) % length

        up_act = dot_f32(full_pair[0], tokens, 1, 1) * up_col
        gate_act = dot_f32(full_pair[1], tokens, 1, 1) * gate_col
        shifted = [later(up_act, TAPS - 1 - k, position) for k in range(TAPS)]
        conv_out = bias_col
        for k in range(TAPS):
            conv_out = conv_out + shifted[k] * column(taps[k])
        gelu_val, gelu_back = jax.vjp(jax.nn.gelu, conv_out)
        hidden = (gelu_val * gate_act).astype(bf16)

        def scatter(term):
            return lax.psum_scatter(term.astype(bf16), "fz", scatter_dimension=1, tiled=True)

        def finish(block):
            return in_order(mine(block, 1), swap(theirs(block, 1)), 0).astype(jnp.float32)

        grad_down = finish(scatter(dot_f32(hidden, scaled_cot, 1, 0)))
        hidden_cot = dot_f32(full_down, scaled_cot, 1, 1)
        gate_cot = (hidden_cot * gelu_val * gate_col).astype(bf16)
        grad_gate = finish(scatter(dot_f32(gate_cot, tokens, 1, 0))).T
        (conv_cot,) = gelu_back(hidden_cot * gate_act)
        act_cot = jnp.zeros_like(conv_cot)
        for k in range(TAPS):
            act_cot = act_cot + column(taps[k]) * earlier(conv_cot, TAPS - 1 - k, position, length)
        up_cot = (act_cot * up_col).astype(bf16)
        grad_up = finish(scatter(dot_f32(up_cot, tokens, 1, 0))).T

        def input_part(start):
            up_side = dot_f32(up_cot[:, start : start + length], full_pair[0], 0, 0)
            return up_side + dot_f32(gate_cot[:, start : start + length], full_pair[1], 0, 0)

        other_part = swap(input_part(length).astype(bf16))
        partial = (input_part(0) + other_part.astype(jnp.float32)).astype(bf16)
        grad_input = sum_over_tp(partial, n_tp)

        sums = [jnp.sum(conv_cot * shifted[k], axis=1) for k in range(TAPS)]
        sums = jnp.stack(sums + [jnp.sum(conv_cot, axis=1)])
        sums = sum_over_fz(sums, n_fz)
        sums = in_order(sums, swap(sums), 1)
        return (grad_input, grad_up, grad_gate, grad_down, sums[:TAPS], sums[TAPS])

    return on_device


def solution(mesh):
    n_fs, n_tp = mesh.shape["fs"], mesh.shape["tp"]
    split = Mesh(mesh.devices.reshape(n_fs // 2, 2, n_tp), ("fz", "fx", "tp"))
    fs = ("fz", "fx")
    in_specs = (
        P(fs, None),
        P(fs, None),
        P(fs, "tp"),
        P(fs, "tp"),
        P("tp", fs),
        P("tp"),
        P("tp"),
        P(),
        P(None, "tp"),
        P("tp"),
    )
    out_specs = (P(fs, None), P(fs, "tp"), P(fs, "tp"), P("tp", fs), P(None, "tp"), P("tp"))
    return jax.shard_map(
        make_on_device(n_fs // 2, n_tp),
        mesh=split,
        in_specs=in_specs,
        out_specs=out_specs,
        check_vma=False,
    )
```

time: 524 us -> 252 us (0.48)
  local copies, waits for them, and re-layouts: 106 us -> 4.99 us
  blocking collectives: 96.4 us -> 0 us
  other arithmetic: 89.6 us -> 19 us
  waiting for transfers between devices: 178 us -> 159 us
  starting transfers between devices: 9.21 us -> 23.3 us
    psum x1 -> x0, blocking collectives: 96.4 us -> none  [on_device(): grad_conv, grad_bias = lax.psum((tap_part, bias_part), 'fs')]
    all_gather x2, waiting for transfers between devices: 155 us -> 60.8 us  [gather(): return lax.all_gather(block, 'fz', axis=2, tiled=True)]
    unnamed x2 -> x0, other arithmetic: 72.6 us -> none
    ppermute x0 -> x17, waiting for transfers between devices: none -> 65.2 us  [the longest x9 49.9 us: swap(): return lax.ppermute(value, 'fx', [(0, 1), (1, 0)])]
    unnamed x30 -> x33, local copies, waits for them, and re-layouts: 44.1 us -> 3.68 us
    reduce_scatter x1 -> x3, waiting for transfers between devices: 0.01 us -> 33.1 us  [scatter(): lax.psum_scatter(term.astype(bf16), 'fz', scatter_dimension=1, tiled=True)]
    convert_element_type x2 -> x0, local copies, waits for them, and re-layouts: 31.5 us -> none  [the longest x1 15.8 us: on_device(): gate_term[None].astype(jnp.bfloat16)]
    all_to_all x2 -> x0, local copies, waits for them, and re-layouts: 30.6 us -> none  [the longest x1 15.3 us: on_device(): lax.all_to_all(gate_term[None].astype(jnp.bfloat16), 'fs', split_axis=1,...]
  transfers between devices with their start and end apart: 6 -> 22, of which waited for: 3 -> 14; matrix products, arithmetic and copies ran while one was open for 28% -> 15% of each run, Pallas kernels for 0% -> 0%
where the time goes in v1:
time: 252 us
  waiting for transfers between devices  159 us (63%)
  matrix products  31.1 us (12%)
  starting transfers between devices  23.3 us (9%)
  other arithmetic  19 us (8%)
  between operations  14.1 us (6%)
  local copies, waits for them, and re-layouts  4.99 us (2%)
    all_gather x2, waiting for transfers between devices, gather(): return lax.all_gather(block, 'fz', axis=2, tiled=True)  60.8 us
    ppermute x9, waiting for transfers between devices, swap(): return lax.ppermute(value, 'fx', [(0, 1), (1, 0)])  49.9 us
    reduce_scatter x3, waiting for transfers between devices, scatter(): lax.psum_scatter(term.astype(bf16), 'fz', scatter_dimension=1, tiled=True)  33.1 us
    dot_general x10, matrix products, dot_f32(): lax.dot_general(left, right, (((left_dim,), (right_dim,)), ((), ())), pre...  31.1 us
    ppermute x9, starting transfers between devices, swap(): return lax.ppermute(value, 'fx', [(0, 1), (1, 0)])  14.5 us
    ppermute x3, waiting for transfers between devices, sum_over_tp(): got = lax.ppermute(own, 'tp', ring)  8.67 us
  transfers between devices with their start and end apart: 22, of which 14 were waited for; matrix products, arithmetic and copies ran while one was open for 15% of the time, Pallas kernels for 0%

profile of v1, /device:TPU:0, one launch (start us, length us, event | category | flops | bytes accessed | tf_op | source)
XLA Modules:
  0.0 251.7 jit_solution(272498820663576095)
XLA Ops:
  7.2 1.4 convert_bitcast_fusion.2
  8.8 3.0 %collective-permute-start.2 = (bf16[2,368,256]{2,1,0:T(8,128)(2,1)S(1)}, bf16[2,368,256]{2,1,0:T(8,128)(2,1)S(1)}, u32[]{:S(2)}, u32[]{:S(2)}) collective-permute-start(bf16[2,368,256]{2,1,0:T(8,128)(2,1)S(1)} %broadcast_select_fusion.2), channel_id=1, source_target_pairs={{0,4},{4,0},{1,5},{5,1},{2,6},{6,2},{3,7},{7,3},{8,12},{12,8},{9,1... | collective-permute-start | bytes 1130504 | tf_op jit(solution)/shard_map/ppermute | solution.py:17
  11.8 8.8 %collective-permute-done.2 = bf16[2,368,256]{2,1,0:T(8,128)(2,1)S(1)} collective-permute-done((bf16[2,368,256]{2,1,0:T(8,128)(2,1)S(1)}, bf16[2,368,256]{2,1,0:T(8,128)(2,1)S(1)}, u32[]{:S(2)}, u32[]{:S(2)}) %collective-permute-start.2) | collective-permute-done | bytes 376864 | tf_op jit(solution)/shard_map/ppermute | solution.py:17
  21.9 1.8 collective-permute-start
  24.0 5.6 %collective-permute-done = bf16[1,368,256]{2,1,0:T(8,128)(2,1)S(1)} collective-permute-done((bf16[1,368,256]{2,1,0:T(8,128)(2,1)S(1)}, bf16[1,368,256]{2,1,0:T(8,128)(2,1)S(1)}, u32[]{:S(2)}, u32[]{:S(2)}) %collective-permute-start) | collective-permute-done | bytes 188448 | tf_op jit(solution)/shard_map/ppermute | solution.py:17
  30.4 1.2 multiply_convert_fusion
  31.6 1.7 collective-permute-start.1
  33.6 1.0 constant_dynamic-update-slice_fusion.1
  34.7 17.3 %collective-permute-done.3 = bf16[256,2048]{1,0:T(8,128)(2,1)S(1)} collective-permute-done((bf16[256,2048]{1,0:T(8,128)(2,1)S(1)}, bf16[256,2048]{1,0:T(8,128)(2,1)S(1)}, u32[]{:S(2)}, u32[]{:S(2)}) %collective-permute-start.3) | collective-permute-done | bytes 1048608 | tf_op jit(solution)/shard_map/ppermute | solution.py:17
  52.0 1.0 constant_dynamic-update-slice_fusion
  53.1 31.6 %all-gather.5.cloned.1.call-done = bf16[2,368,2048]{2,1,0:T(8,128)(2,1)} async-done(((bf16[2,368,512]{2,1,0:T(8,128)(2,1)}), bf16[2,368,2048]{2,1,0:T(8,128)(2,1)}) %all-gather.5.cloned.1.call-update) | async-done | bytes 3014672 | tf_op jit(solution)/shard_map/all_gather | solution.py:105
  84.6 4.0 %convolution_multiply_fusion.1 = f32[368,512]{1,0:T(8,128)} fusion(bf16[512,2048]{1,0:T(8,128)(2,1)} %constant_dynamic-update-slice_fusion, bf16[2,368,2048]{2,1,0:T(8,128)(2,1)} %all-gather.5.cloned.1.call-done, f32[368]{0:T(512)S(1)} %slice_select_fusion.3), kind=kOutput, calls=%fused_computation.14 | convolution fusion | flops 771940352 | bytes 4359616 | tf_op jit(solution)/shard_map/dot_general | solution.py:11
  88.7 3.4 %convolution_multiply_fusion = f32[368,512]{1,0:T(8,128)} fusion(bf16[512,2048]{1,0:T(8,128)(2,1)} %constant_dynamic-update-slice_fusion, bf16[2,368,2048]{2,1,0:T(8,128)(2,1)S(1)} %copy-done, f32[368]{0:T(512)S(1)} %get-tuple-element.37), kind=kOutput, calls=%fused_computation.13 | convolution fusion | flops 771940352 | bytes 4360192 | tf_op jit(solution)/shard_map/dot_general | solution.py:11
  92.1 29.3 %all-gather.3.cloned.1.call-done = bf16[1,368,2048]{2,1,0:T(8,128)(2,1)} async-done(((bf16[1,368,512]{2,1,0:T(8,128)(2,1)}), bf16[1,368,2048]{2,1,0:T(8,128)(2,1)}) %all-gather.3.cloned.1.call-update) | async-done | bytes 1507344 | tf_op jit(solution)/shard_map/all_gather | solution.py:105
  121.4 6.3 %multiply_reduce_fusion.2 = (f32[368]{0:T(512)S(1)}, f32[368]{0:T(512)S(1)}, f32[368]{0:T(512)S(1)}, f32[368]{0:T(512)S(1)}, f32[368,512]{1,0:T(8,128)}, /*index=5*/f32[368,512]{1,0:T(8,128)S(1)}, f32[368,512]{1,0:T(8,128)}) fusion(f32[368,512]{1,0:T(8,128)} %convolution_multiply_fusion, pred[512]{0:T(512)(128)(4,1)S(1)} %get-tuple-element.35, ...), kind=kOutput, calls=%fused_computation.46 | convolution fusion | flops 782916096 | bytes 7385600 | tf_op jit(solution)/shard_map/dot_general | solution.py:11
  128.6 3.8 %convolution_convert_fusion = bf16[368,2048]{1,0:T(8,128)(2,1)} fusion(bf16[256,2048]{1,0:T(8,128)(2,1)} %collective-permute-done.1, bf16[256,2048]{1,0:T(8,128)(2,1)} %multiply_convert_fusion, f32[368,512]{1,0:T(8,128)S(1)} %copy-done.15, f32[368,512]{1,0:T(8,128)S(1)} %get-tuple-element.14), kind=kOutput, calls=%fused_computation | convolution fusion | flops 778584064 | bytes 5111808 | tf_op jit(solution)/shard_map/dot_general | solution.py:11
  132.4 1.6 multiply_convert_fusion.2
  134.0 3.7 %convolution_convert_fusion.1 = bf16[368,2048]{1,0:T(8,128)(2,1)} fusion(bf16[368,512]{1,0:T(8,128)(2,1)S(1)} %multiply_convert_fusion.2, bf16[512,2048]{1,0:T(8,128)(2,1)} %constant_dynamic-update-slice_fusion), kind=kOutput, calls=%fused_computation.1 | convolution fusion | flops 772505600 | bytes 3981312 | tf_op jit(solution)/shard_map/dot_general | solution.py:11
  137.8 2.5 fusion.12
  141.8 1.7 fusion
  143.5 1.5 collective-permute-start.4
  145.7 3.8 %convolution_convert_fusion.2 = bf16[368,2048]{1,0:T(8,128)(2,1)} fusion(bf16[368,512]{1,0:T(8,128)(2,1)} %copy-done.4, bf16[512,2048]{1,0:T(8,128)(2,1)} %constant_dynamic-update-slice_fusion), kind=kOutput, calls=%fused_computation.2 | convolution fusion | flops 772505600 | bytes 3981312 | tf_op jit(solution)/shard_map/dot_general | solution.py:11
  149.6 1.7 fusion.4
  151.2 16.6 %collective-permute-done.4 = bf16[256,2048]{1,0:T(8,128)(2,1)} collective-permute-done((bf16[256,2048]{1,0:T(8,128)(2,1)}, bf16[256,2048]{1,0:T(8,128)(2,1)}, u32[]{:S(2)}, u32[]{:S(2)}) %collective-permute-start.4) | collective-permute-done | bytes 1048608 | tf_op jit(solution)/shard_map/ppermute | solution.py:17
  167.9 2.0 add_convert_fusion
  169.9 1.0 copy-done.1
  171.0 1.5 collective-permute-start.6
  172.5 1.4 collective-permute-start.7
  173.9 2.0 collective-permute-start.15
  176.0 2.9 %collective-permute-done.15 = f32[4,368]{1,0:T(4,128)S(1)} collective-permute-done((f32[4,368]{1,0:T(4,128)S(1)}, f32[4,368]{1,0:T(4,128)S(1)}, u32[]{:S(2)}, u32[]{:S(2)}) %collective-permute-start.15) | collective-permute-done | bytes 5920 | tf_op jit(solution)/shard_map/ppermute | solution.py:43
  178.9 1.5 collective-permute-start.16
  180.5 3.7 %collective-permute-done.7 = bf16[64,2048]{1,0:T(8,128)(2,1)S(1)} collective-permute-done((bf16[64,2048]{1,0:T(8,128)(2,1)S(1)}, bf16[64,2048]{1,0:T(8,128)(2,1)S(1)}, u32[]{:S(2)}, u32[]{:S(2)}) %collective-permute-start.7) | collective-permute-done | bytes 262176 | tf_op jit(solution)/shard_map/ppermute | solution.py:58
  184.3 1.1 constant_dynamic-update-slice_fusion.5
  185.4 1.3 collective-permute-start.8
  186.7 1.5 collective-permute-start.9
  189.6 3.7 %collective-permute-done.8 = bf16[64,2048]{1,0:T(8,128)(2,1)S(1)} collective-permute-done((bf16[64,2048]{1,0:T(8,128)(2,1)S(1)}, bf16[64,2048]{1,0:T(8,128)(2,1)S(1)}, u32[]{:S(2)}, u32[]{:S(2)}) %collective-permute-start.8) | collective-permute-done | bytes 262176 | tf_op jit(solution)/shard_map/ppermute | solution.py:64
  193.3 2.6 %collective-permute-done.9 = bf16[64,2048]{1,0:T(8,128)(2,1)S(1)} collective-permute-done((bf16[64,2048]{1,0:T(8,128)(2,1)S(1)}, bf16[64,2048]{1,0:T(8,128)(2,1)S(1)}, u32[]{:S(2)}, u32[]{:S(2)}) %collective-permute-start.9) | collective-permute-done | bytes 262176 | tf_op jit(solution)/shard_map/ppermute | solution.py:64
  195.9 2.4 collective-permute-done.10
  198.4 1.4 broadcast_select_fusion.6
  199.8 1.5 collective-permute-start.13
  201.5 1.1 broadcast_select_fusion.10
  202.6 1.5 collective-permute-start.12
  204.1 32.9 %reduce-scatter.4.cloned.1.call-done = bf16[368,512]{1,0:T(8,128)(2,1)} async-done(((bf16[368,2048]{1,0:T(8,128)(2,1)}), bf16[368,512]{1,0:T(8,128)(2,1)}) %reduce-scatter.4.cloned.1.call-update) | async-done | bytes 376848 | tf_op jit(solution)/shard_map/reduce_scatter | solution.py:128
  237.0 1.0 broadcast_select_fusion.14
  238.0 1.5 collective-permute-start.11
  239.6 1.1 broadcast_select_fusion.5
  240.7 0.9 maximum_convert_fusion
  242.6 1.6 collective-permute-done.11
  (87 shorter events, 9.9 us)
Async XLA Ops:
  7.2 77.5 %all-gather.5.cloned.1.call-start = ((), (), s32[]{:S(2)}) async-start(), calls=%async_computation.4 | async-start | bytes 3768320 | tf_op jit(solution)/shard_map/all_gather | solution.py:105
  8.7 13.0 %copy-start.8 = (f32[736,256]{1,0:T(8,128)S(1)}, f32[736,256]{1,0:T(8,128)}, u32[]{:S(2)}) copy-start(f32[736,256]{1,0:T(8,128)} %param.14) | copy-start | bytes 2260996
  8.8 11.8 %collective-permute-start.2 = (bf16[2,368,256]{2,1,0:T(8,128)(2,1)S(1)}, bf16[2,368,256]{2,1,0:T(8,128)(2,1)S(1)}, u32[]{:S(2)}, u32[]{:S(2)}) collective-permute-start(bf16[2,368,256]{2,1,0:T(8,128)(2,1)S(1)} %broadcast_select_fusion.2), channel_id=1, source_target_pairs={{0,4},{4,0},{1,5},{5,1},{2,6},{6,2},{3,7},{7,3},{8,12},{12,8},{9,1... | collective-permute-start | bytes 1130504 | tf_op jit(solution)/shard_map/ppermute | solution.py:17
  20.7 3.0 %copy-start.6 = (bf16[256,2048]{1,0:T(8,128)(2,1)S(1)}, bf16[256,2048]{1,0:T(8,128)(2,1)}, u32[]{:S(2)}) copy-start(bf16[256,2048]{1,0:T(8,128)(2,1)} %param.10) | copy-start | bytes 3145732
  21.7 8.8 %copy-start.5 = (bf16[256,2048]{1,0:T(8,128)(2,1)S(1)}, bf16[256,2048]{1,0:T(8,128)(2,1)}, u32[]{:S(2)}) copy-start(bf16[256,2048]{1,0:T(8,128)(2,1)} %param.11) | copy-start | bytes 3145732
  21.7 8.8 %copy-start.11 = (f32[2048]{0:T(1024)S(1)}, f32[2048]{0:T(1024)}, u32[]{:S(2)}) copy-start(f32[2048]{0:T(1024)} %param.17) | copy-start | bytes 24580
  21.7 99.7 %all-gather.3.cloned.1.call-start = ((), (), s32[]{:S(2)}) async-start(), calls=%async_computation.3 | async-start | bytes 1884160 | tf_op jit(solution)/shard_map/all_gather | solution.py:105
  21.8 11.6 %copy-start.10 = (f32[3,736]{1,0:T(4,128)S(1)}, f32[3,736]{1,0:T(4,128)}, u32[]{:S(2)}) copy-start(f32[3,736]{1,0:T(4,128)} %param.18) | copy-start | bytes 26500
  21.8 11.7 %copy-start.14 = (f32[736]{0:T(1024)S(1)}, f32[736]{0:T(1024)}, u32[]{:S(2)}) copy-start(f32[736]{0:T(1024)} %param.16) | copy-start | bytes 8836
  21.9 11.7 %copy-start.12 = (f32[736]{0:T(1024)S(1)}, f32[736]{0:T(1024)}, u32[]{:S(2)}) copy-start(f32[736]{0:T(1024)} %param.15) | copy-start | bytes 8836
  21.9 11.7 %copy-start.13 = (f32[736]{0:T(1024)S(1)}, f32[736]{0:T(1024)}, u32[]{:S(2)}) copy-start(f32[736]{0:T(1024)} %param.19) | copy-start | bytes 8836
  21.9 7.7 %collective-permute-start = (bf16[1,368,256]{2,1,0:T(8,128)(2,1)S(1)}, bf16[1,368,256]{2,1,0:T(8,128)(2,1)S(1)}, u32[]{:S(2)}, u32[]{:S(2)}) collective-permute-start(bf16[1,368,256]{2,1,0:T(8,128)(2,1)S(1)} %broadcast_select_fusion.18), channel_id=1, source_target_pairs={{0,4},{4,0},{1,5},{5,1},{2,6},{6,2},{3,7},{7,3},{8,12},{12,8},{9,1... | collective-permute-start | bytes 565256 | tf_op jit(solution)/shard_map/ppermute | solution.py:17
  23.7 28.3 %collective-permute-start.3 = (bf16[256,2048]{1,0:T(8,128)(2,1)S(1)}, bf16[256,2048]{1,0:T(8,128)(2,1)S(1)}, u32[]{:S(2)}, u32[]{:S(2)}) collective-permute-start(bf16[256,2048]{1,0:T(8,128)(2,1)S(1)} %copy-done.6), channel_id=1, source_target_pairs={{0,4},{4,0},{1,5},{5,1},{2,6},{6,2},{3,7},{7,3},{8,12},{12,8},{9,1... | collective-permute-start | bytes 3145736 | tf_op jit(solution)/shard_map/ppermute | solution.py:17
  30.4 168.0 %reduce-scatter.8.cloned.1.call-start = ((), (), s32[]{:S(2)}) async-start(), calls=%async_computation.7 | async-start | bytes 1884160 | tf_op jit(solution)/shard_map/reduce_scatter | solution.py:128
  31.6 60.5 %collective-permute-start.1 = (bf16[256,2048]{1,0:T(8,128)(2,1)}, bf16[256,2048]{1,0:T(8,128)(2,1)}, u32[]{:S(2)}, u32[]{:S(2)}) collective-permute-start(bf16[256,2048]{1,0:T(8,128)(2,1)} %multiply_convert_fusion), channel_id=1, source_target_pairs={{0,4},{4,0},{1,5},{5,1},{2,6},{6,2},{3,7},{7,3},{8,12},{12,8},{9,1... | collective-permute-start | bytes 3145736 | tf_op jit(solution)/shard_map/ppermute | solution.py:17
  84.6 4.0 %copy-start = (bf16[2,368,2048]{2,1,0:T(8,128)(2,1)S(1)}, bf16[2,368,2048]{2,1,0:T(8,128)(2,1)}, u32[]{:S(2)}) copy-start(bf16[2,368,2048]{2,1,0:T(8,128)(2,1)} %all-gather.5.cloned.1.call-done) | copy-start | bytes 9043972
  121.4 7.2 %copy-start.15 = (f32[368,512]{1,0:T(8,128)S(1)}, f32[368,512]{1,0:T(8,128)}, u32[]{:S(2)}) copy-start(f32[368,512]{1,0:T(8,128)} %convolution_multiply_fusion.1) | copy-start | bytes 2260996
  127.7 0.9 copy-start.9
  132.4 69.1 %reduce-scatter.6.cloned.1.call-start = ((), (), s32[]{:S(2)}) async-start(), calls=%async_computation.6 | async-start | bytes 1884160 | tf_op jit(solution)/shard_map/reduce_scatter | solution.py:128
  137.7 99.3 %reduce-scatter.4.cloned.1.call-start = ((), (), s32[]{:S(2)}) async-start(), calls=%async_computation.5 | async-start | bytes 1884160 | tf_op jit(solution)/shard_map/reduce_scatter | solution.py:128
  140.3 0.7 copy-start.4
  143.5 24.4 %collective-permute-start.4 = (bf16[256,2048]{1,0:T(8,128)(2,1)}, bf16[256,2048]{1,0:T(8,128)(2,1)}, u32[]{:S(2)}, u32[]{:S(2)}) collective-permute-start(bf16[256,2048]{1,0:T(8,128)(2,1)} %fusion), channel_id=1, source_target_pairs={{0,4},{4,0},{1,5},{5,1},{2,6},{6,2},{3,7},{7,3},{8,12},{12,8},{9,1... | collective-permute-start | bytes 3145736 | tf_op jit(solution)/shard_map/ppermute | solution.py:17
  145.0 28.9 %collective-permute-start.14 = (f32[4,368]{1,0:T(4,128)S(1)}, f32[4,368]{1,0:T(4,128)S(1)}, u32[]{:S(2)}, u32[]{:S(2)}) collective-permute-start(f32[4,368]{1,0:T(4,128)S(1)} %pad_maximum_fusion.6), channel_id=1, source_target_pairs={{0,8},{8,0},{16,24},{24,16},{1,9},{9,1},{17,25},{25,17},{2,10},{10... | collective-permute-start | bytes 17672 | tf_op jit(solution)/shard_map/ppermute | solution.py:43
  169.9 1.0 copy-start.1
  170.9 9.6 %collective-permute-start.5 = (bf16[64,2048]{1,0:T(8,128)(2,1)S(1)}, bf16[64,2048]{1,0:T(8,128)(2,1)S(1)}, u32[]{:S(2)}, u32[]{:S(2)}) collective-permute-start(bf16[64,2048]{1,0:T(8,128)(2,1)S(1)} %get-tuple-element.19), channel_id=1, source_target_pairs={{0,1},{1,2},{2,3},{3,0},{4,5},{5,6},{6,7},{7,4},{8,9},{9,10},{10,1... | collective-permute-start | bytes 786440 | tf_op jit(solution)/shard_map/ppermute | solution.py:58
  171.0 9.5 %collective-permute-start.6 = (bf16[64,2048]{1,0:T(8,128)(2,1)S(1)}, bf16[64,2048]{1,0:T(8,128)(2,1)S(1)}, u32[]{:S(2)}, u32[]{:S(2)}) collective-permute-start(bf16[64,2048]{1,0:T(8,128)(2,1)S(1)} %get-tuple-element.21), channel_id=1, source_target_pairs={{0,2},{1,3},{2,0},{3,1},{4,6},{5,7},{6,4},{7,5},{8,10},{9,11},{10,... | collective-permute-start | bytes 786440 | tf_op jit(solution)/shard_map/ppermute | solution.py:58
  172.5 11.7 %collective-permute-start.7 = (bf16[64,2048]{1,0:T(8,128)(2,1)S(1)}, bf16[64,2048]{1,0:T(8,128)(2,1)S(1)}, u32[]{:S(2)}, u32[]{:S(2)}) collective-permute-start(bf16[64,2048]{1,0:T(8,128)(2,1)S(1)} %get-tuple-element.20), channel_id=1, source_target_pairs={{0,3},{1,0},{2,1},{3,2},{4,7},{5,4},{6,5},{7,6},{8,11},{9,8},{10,9... | collective-permute-start | bytes 786440 | tf_op jit(solution)/shard_map/ppermute | solution.py:58
  173.9 5.0 %collective-permute-start.15 = (f32[4,368]{1,0:T(4,128)S(1)}, f32[4,368]{1,0:T(4,128)S(1)}, u32[]{:S(2)}, u32[]{:S(2)}) collective-permute-start(f32[4,368]{1,0:T(4,128)S(1)} %fusion.40), channel_id=1, source_target_pairs={{0,16},{8,24},{16,0},{24,8},{1,17},{9,25},{17,1},{25,9},{2,18},{10... | collective-permute-start | bytes 17672 | tf_op jit(solution)/shard_map/ppermute | solution.py:43
  178.9 7.7 %collective-permute-start.16 = (f32[4,368]{1,0:T(4,128)S(1)}, f32[4,368]{1,0:T(4,128)S(1)}, u32[]{:S(2)}, u32[]{:S(2)}) collective-permute-start(f32[4,368]{1,0:T(4,128)S(1)} %fusion.48), channel_id=1, source_target_pairs={{0,4},{4,0},{1,5},{5,1},{2,6},{6,2},{3,7},{7,3},{8,12},{12,8},{9,1... | collective-permute-start | bytes 17672 | tf_op jit(solution)/shard_map/ppermute | solution.py:17
  185.4 7.9 %collective-permute-start.8 = (bf16[64,2048]{1,0:T(8,128)(2,1)S(1)}, bf16[64,2048]{1,0:T(8,128)(2,1)S(1)}, u32[]{:S(2)}, u32[]{:S(2)}) collective-permute-start(bf16[64,2048]{1,0:T(8,128)(2,1)S(1)} %get-tuple-element.16), channel_id=1, source_target_pairs={{0,1},{1,2},{2,3},{3,0},{4,5},{5,6},{6,7},{7,4},{8,9},{9,10},{10,1... | collective-permute-start | bytes 786440 | tf_op jit(solution)/shard_map/ppermute | solution.py:64
  186.7 9.2 %collective-permute-start.9 = (bf16[64,2048]{1,0:T(8,128)(2,1)S(1)}, bf16[64,2048]{1,0:T(8,128)(2,1)S(1)}, u32[]{:S(2)}, u32[]{:S(2)}) collective-permute-start(bf16[64,2048]{1,0:T(8,128)(2,1)S(1)} %get-tuple-element.16), channel_id=1, source_target_pairs={{0,2},{1,3},{2,0},{3,1},{4,6},{5,7},{6,4},{7,5},{8,10},{9,11},{10,... | collective-permute-start | bytes 786440 | tf_op jit(solution)/shard_map/ppermute | solution.py:64
  189.6 8.7 %collective-permute-start.10 = (bf16[64,2048]{1,0:T(8,128)(2,1)S(1)}, bf16[64,2048]{1,0:T(8,128)(2,1)S(1)}, u32[]{:S(2)}, u32[]{:S(2)}) collective-permute-start(bf16[64,2048]{1,0:T(8,128)(2,1)S(1)} %get-tuple-element.16), channel_id=1, source_target_pairs={{0,3},{1,0},{2,1},{3,2},{4,7},{5,4},{6,5},{7,6},{8,11},{9,8},{10,9... | collective-permute-start | bytes 786440 | tf_op jit(solution)/shard_map/ppermute | solution.py:64
  198.3 43.3 %copy-start.7 = (bf16[256,2048]{1,0:T(8,128)(2,1)}, bf16[256,2048]{1,0:T(8,128)(2,1)S(1)}, u32[]{:S(2)}) copy-start(bf16[256,2048]{1,0:T(8,128)(2,1)S(1)} %constant_dynamic-update-slice_fusion.2) | copy-start | bytes 3145732
  199.8 39.8 %collective-permute-start.13 = (bf16[368,256]{1,0:T(8,128)(2,1)S(1)}, bf16[368,256]{1,0:T(8,128)(2,1)S(1)}, u32[]{:S(2)}, u32[]{:S(2)}) collective-permute-start(bf16[368,256]{1,0:T(8,128)(2,1)S(1)} %broadcast_select_fusion.6), channel_id=1, source_target_pairs={{0,4},{4,0},{1,5},{5,1},{2,6},{6,2},{3,7},{7,3},{8,12},{12,8},{9,1... | collective-permute-start | bytes 565256 | tf_op jit(solution)/shard_map/ppermute | solution.py:17
  201.5 39.2 %copy-start.2 = (bf16[368,512]{1,0:T(8,128)(2,1)S(1)}, bf16[368,512]{1,0:T(8,128)(2,1)}, u32[]{:S(2)}) copy-start(bf16[368,512]{1,0:T(8,128)(2,1)} %reduce-scatter.6.cloned.1.call-done) | copy-start | bytes 1130500
  202.6 38.1 %collective-permute-start.12 = (bf16[368,256]{1,0:T(8,128)(2,1)S(1)}, bf16[368,256]{1,0:T(8,128)(2,1)S(1)}, u32[]{:S(2)}, u32[]{:S(2)}) collective-permute-start(bf16[368,256]{1,0:T(8,128)(2,1)S(1)} %broadcast_select_fusion.10), channel_id=1, source_target_pairs={{0,4},{4,0},{1,5},{5,1},{2,6},{6,2},{3,7},{7,3},{8,12},{12,8},{9,1... | collective-permute-start | bytes 565256 | tf_op jit(solution)/shard_map/ppermute | solution.py:17
  238.0 6.2 %copy-start.3 = (bf16[368,512]{1,0:T(8,128)(2,1)S(1)}, bf16[368,512]{1,0:T(8,128)(2,1)}, u32[]{:S(2)}) copy-start(bf16[368,512]{1,0:T(8,128)(2,1)} %reduce-scatter.4.cloned.1.call-done) | copy-start | bytes 1130500
  238.0 6.1 %collective-permute-start.11 = (bf16[368,256]{1,0:T(8,128)(2,1)S(1)}, bf16[368,256]{1,0:T(8,128)(2,1)S(1)}, u32[]{:S(2)}, u32[]{:S(2)}) collective-permute-start(bf16[368,256]{1,0:T(8,128)(2,1)S(1)} %broadcast_select_fusion.14), channel_id=1, source_target_pairs={{0,4},{4,0},{1,5},{5,1},{2,6},{6,2},{3,7},{7,3},{8,12},{12,8},{9,1... | collective-permute-start | bytes 565256 | tf_op jit(solution)/shard_map/ppermute | solution.py:17
Sparse Core Ops, SparseCore 0:
  21.8 62.7 all-gather.4
  86.8 34.5 all-gather.2
  132.5 33.4 reduce-scatter.7
  168.2 33.2 reduce-scatter.5
  203.6 33.2 reduce-scatter.3

commit v2 on v1

--- a/solution.py
+++ b/solution.py
@@ -83,7 +83,6 @@
         bf16 = jnp.bfloat16
         low = lax.axis_index("fx") == 0
         length = inputs.shape[0]
-        half = down_weight.shape[0] // 2
         width = down_weight.shape[1]
 
         def mine(value, axis=0):
@@ -99,14 +98,31 @@
                 [jnp.where(low, own, other), jnp.where(low, other, own)], axis=axis
             )
 
-        def gather(weights):
-            stored = jnp.stack([w.astype(bf16) for w in weights])
-            block = in_order(mine(stored, 1), swap(theirs(stored, 1)), 2)
-            return lax.all_gather(block, "fz", axis=2, tiled=True)
-
-        full_pair = gather([up_weight.T, gate_weight.T])
-        full_down = gather([down_weight])[0]
+        def gather(block):
+            return lax.all_gather(block, "fz", axis=block.ndim - 1, tiled=True)
+
+        pair = jnp.stack([up_weight.T.astype(bf16), gate_weight.T.astype(bf16)])
+        own_pair = gather(mine(pair, 1))
+        other_pair = gather(swap(theirs(pair, 1)))
+        stored_down = down_weight.astype(bf16)
+        full_down = gather(in_order(mine(stored_down), swap(theirs(stored_down)), 1))
+        first_pair = jnp.where(low, own_pair, other_pair)
+        second_pair = jnp.where(low, other_pair, own_pair)
+        full_pair = jnp.concatenate(
+            [
+                block[:, :, i * width : (i + 1) * width]
+                for i in range(n_fz)
+                for block in (first_pair, second_pair)
+            ],
+            axis=2,
+        )
         tokens = jnp.concatenate([inputs, swap(inputs)], axis=0)
+        even_rows = [tokens[:, 2 * i * width : (2 * i + 1) * width] for i in range(n_fz)]
+        odd_rows = [tokens[:, (2 * i + 1) * width : (2 * i + 2) * width] for i in range(n_fz)]
+        even_rows = jnp.concatenate(even_rows, axis=1)
+        odd_rows = jnp.concatenate(odd_rows, axis=1)
+        own_rows = jnp.where(low, even_rows, odd_rows)
+        other_rows = jnp.where(low, odd_rows, even_rows)
         scaled_own = (cotangent.astype(jnp.float32) * down_scale).astype(bf16)
         scaled_cot = jnp.concatenate([scaled_own, swap(scaled_own)], axis=0)
         up_col = column(mine(up_scale))
@@ -130,16 +146,24 @@
         def finish(block):
             return in_order(mine(block, 1), swap(theirs(block, 1)), 0).astype(jnp.float32)
 
-        grad_down = finish(scatter(dot_f32(hidden, scaled_cot, 1, 0)))
+        hidden = lax.optimization_barrier(hidden)
+        down_term = dot_f32(hidden, scaled_cot, 1, 0).astype(bf16)
+        down_term, scaled_cot = lax.optimization_barrier((down_term, scaled_cot))
+        grad_down = finish(scatter(down_term))
         hidden_cot = dot_f32(full_down, scaled_cot, 1, 1)
         gate_cot = (hidden_cot * gelu_val * gate_col).astype(bf16)
-        grad_gate = finish(scatter(dot_f32(gate_cot, tokens, 1, 0))).T
         (conv_cot,) = gelu_back(hidden_cot * gate_act)
         act_cot = jnp.zeros_like(conv_cot)
         for k in range(TAPS):
             act_cot = act_cot + column(taps[k]) * earlier(conv_cot, TAPS - 1 - k, position, length)
         up_cot = (act_cot * up_col).astype(bf16)
-        grad_up = finish(scatter(dot_f32(up_cot, tokens, 1, 0))).T
+        cots = jnp.concatenate([gate_cot, up_cot], axis=0)
+        sent = scatter(dot_f32(cots, other_rows, 1, 0))
+        kept = scatter(dot_f32(cots, own_rows, 1, 0))
+        received = swap(sent)
+        half = up_cot.shape[0]
+        grad_gate = in_order(kept[:half], received[:half], 0).astype(jnp.float32).T
+        grad_up = in_order(kept[half:], received[half:], 0).astype(jnp.float32).T
 
         def input_part(start):
             up_side = dot_f32(up_cot[:, start : start + length], full_pair[0], 0, 0)

time: 252 us -> 239 us (0.948)
  waiting for transfers between devices: 159 us -> 150 us
  matrix products: 31.1 us -> 22.5 us
  local copies, waits for them, and re-layouts: 4.99 us -> 10 us
    all_gather x2 -> x3, waiting for transfers between devices: 60.8 us -> 30.5 us  [gather(): return lax.all_gather(block, 'fz', axis=block.ndim - 1, tiled=True)]
    ppermute x9 -> x8, waiting for transfers between devices: 49.9 us -> 70.7 us  [swap(): return lax.ppermute(value, 'fx', [(0, 1), (1, 0)])]
    dot_general x10, matrix products: 31.1 us -> 22.5 us  [dot_f32(): lax.dot_general(left, right, (((left_dim,), (right_dim,)), ((), ())), pre...]
    slice x0 -> x1, local copies, waits for them, and re-layouts: none -> 2.97 us  [on_device(): tokens[:, 2 * i * width:(2 * i + 1) * width]]
    reduce_scatter x3, waiting for transfers between devices: 33.1 us -> 35.9 us  [scatter(): lax.psum_scatter(term.astype(bf16), 'fz', scatter_dimension=1, tiled=True)]
    concatenate x0 -> x1, other arithmetic: none -> 2.78 us  [on_device(): scaled_cot = jnp.concatenate([scaled_own, swap(scaled_own)], axis=0)]
    unnamed x33 -> x62, local copies, waits for them, and re-layouts: 3.68 us -> 5.45 us
    ppermute x9 -> x8, starting transfers between devices: 14.5 us -> 13 us  [swap(): return lax.ppermute(value, 'fx', [(0, 1), (1, 0)])]
  transfers between devices with their start and end apart: 22 -> 22, of which waited for: 14 -> 11; matrix products, arithmetic and copies ran while one was open for 15% -> 18% of each run, Pallas kernels for 0% -> 0%
where the time goes in v2:
time: 239 us
  waiting for transfers between devices  150 us (63%)
  matrix products  22.5 us (9%)
  starting transfers between devices  22.1 us (9%)
  other arithmetic  19.3 us (8%)
  between operations  14.7 us (6%)
  local copies, waits for them, and re-layouts  10 us (4%)
    ppermute x8, waiting for transfers between devices, swap(): return lax.ppermute(value, 'fx', [(0, 1), (1, 0)])  70.7 us
    reduce_scatter x3, waiting for transfers between devices, scatter(): lax.psum_scatter(term.astype(bf16), 'fz', scatter_dimension=1, tiled=True)  35.9 us
    all_gather x3, waiting for transfers between devices, gather(): return lax.all_gather(block, 'fz', axis=block.ndim - 1, tiled=True)  30.5 us
    dot_general x10, matrix products, dot_f32(): lax.dot_general(left, right, (((left_dim,), (right_dim,)), ((), ())), pre...  22.5 us
    ppermute x8, starting transfers between devices, swap(): return lax.ppermute(value, 'fx', [(0, 1), (1, 0)])  13 us
    ppermute x3, waiting for transfers between devices, sum_over_tp(): got = lax.ppermute(own, 'tp', ring)  6.33 us
    unnamed x62, local copies, waits for them, and re-layouts  5.45 us
  transfers between devices with their start and end apart: 22, of which 11 were waited for; matrix products, arithmetic and copies ran while one was open for 18% of the time, Pallas kernels for 0%

profile of v2, /device:TPU:0, one launch (start us, length us, event | category | flops | bytes accessed | tf_op | source)
XLA Modules:
  0.0 238.7 jit_solution(11795296588668400917)
XLA Ops:
  7.2 1.5 convert_bitcast_fusion.2
  9.7 3.0 %collective-permute-start.1 = (bf16[2,368,256]{2,1,0:T(8,128)(2,1)S(1)}, bf16[2,368,256]{2,1,0:T(8,128)(2,1)S(1)}, u32[]{:S(2)}, u32[]{:S(2)}) collective-permute-start(bf16[2,368,256]{2,1,0:T(8,128)(2,1)S(1)} %get-tuple-element.40), channel_id=1, source_target_pairs={{0,4},{4,0},{1,5},{5,1},{2,6},{6,2},{3,7},{7,3},{8,12},{12,8},{9,1... | collective-permute-start | bytes 1130504 | tf_op jit(solution)/shard_map/ppermute | solution.py:17
  12.8 8.8 %collective-permute-done.1 = bf16[2,368,256]{2,1,0:T(8,128)(2,1)S(1)} collective-permute-done((bf16[2,368,256]{2,1,0:T(8,128)(2,1)S(1)}, bf16[2,368,256]{2,1,0:T(8,128)(2,1)S(1)}, u32[]{:S(2)}, u32[]{:S(2)}) %collective-permute-start.1) | collective-permute-done | bytes 376864 | tf_op jit(solution)/shard_map/ppermute | solution.py:17
  22.3 1.8 collective-permute-start.2
  24.8 1.8 collective-permute-start
  26.8 1.3 constant_dynamic-update-slice_fusion.1
  28.2 45.2 %collective-permute-done = bf16[368,256]{1,0:T(8,128)(2,1)S(1)} collective-permute-done((bf16[368,256]{1,0:T(8,128)(2,1)S(1)}, bf16[368,256]{1,0:T(8,128)(2,1)S(1)}, u32[]{:S(2)}, u32[]{:S(2)}) %collective-permute-start) | collective-permute-done | bytes 188448 | tf_op jit(solution)/shard_map/ppermute | solution.py:17
  74.4 2.8 %pad_maximum_fusion = bf16[512,2048]{1,0:T(8,128)(2,1)} fusion(bf16[256,2048]{1,0:T(8,128)(2,1)} %collective-permute-done.3, bf16[256,2048]{1,0:T(8,128)(2,1)S(1)} %multiply_convert_fusion), kind=kLoop, calls=%fused_computation.4 | loop fusion | flops 4194304 | bytes 4194304 | tf_op jit(solution)/shard_map/concatenate | solution.py:127
  77.2 1.3 constant_dynamic-update-slice_fusion
  78.5 8.0 %all-gather.8.cloned.1.call-done = bf16[2,368,1024]{2,1,0:T(8,128)(2,1)} async-done(((bf16[2,368,256]{2,1,0:T(8,128)(2,1)}), bf16[2,368,1024]{2,1,0:T(8,128)(2,1)}) %all-gather.8.cloned.1.call-update) | async-done | bytes 1507344 | tf_op jit(solution)/shard_map/all_gather | solution.py:102
  86.5 2.0 broadcast_select_fusion
  89.1 1.2 copy-done.1
  90.3 1.0 convolution_multiply_fusion.1
  91.3 2.1 multiply_convert_fusion.2
  93.4 3.4 %convolution_convert_fusion = bf16[368,2048]{1,0:T(8,128)(2,1)} fusion(bf16[368,512]{1,0:T(8,128)(2,1)S(1)} %get-tuple-element.20, bf16[256,2048]{1,0:T(8,128)(2,1)} %collective-permute-done.3, bf16[256,2048]{1,0:T(8,128)(2,1)S(1)} %copy-done.4), kind=kOutput, calls=%fused_computation | convolution fusion | flops 776699904 | bytes 3981312 | tf_op jit(solution)/shard_map/dot_general | solution.py:11
  96.9 3.0 %fusion.40 = (bf16[512,256]{1,0:T(8,128)(2,1)}, bf16[512,256]{1,0:T(8,128)(2,1)}, bf16[512,256]{1,0:T(8,128)(2,1)}, bf16[512,256]{1,0:T(8,128)(2,1)}, bf16[512,2...) fusion(bf16[512,2048]{1,0:T(8,128)(2,1)} %copy-done), kind=kLoop, calls=%fused_computation.124 | loop fusion | bytes 4194304 | tf_op jit(solution)/shard_map/slice | solution.py:120
  99.8 22.4 %all-gather.4.cloned.1.call-done = bf16[368,2048]{1,0:T(8,128)(2,1)} async-done(((bf16[368,512]{1,0:T(8,128)(2,1)}), bf16[368,2048]{1,0:T(8,128)(2,1)}) %all-gather.4.cloned.1.call-update) | async-done | bytes 1507344 | tf_op jit(solution)/shard_map/all_gather | solution.py:102
  122.2 3.2 %fusion.41 = f32[368,512]{1,0:T(8,128)S(1)} fusion(bf16[368,2048]{1,0:T(8,128)(2,1)} %all-gather.4.cloned.1.call-done, bf16[512,2048]{1,0:T(8,128)(2,1)} %pad_maximum_fusion), kind=kOutput, calls=%fused_computation.125 | convolution fusion | flops 771751936 | bytes 4358144 | tf_op jit(solution)/shard_map/dot_general | solution.py:11
  125.5 1.2 multiply_reduce_fusion.2
  128.3 2.2 convolution_convert_fusion.1
  130.7 1.7 fusion.1
  132.4 1.7 fusion
  134.1 1.5 collective-permute-start.4
  136.3 3.7 %convolution_convert_fusion.2 = bf16[736,1024]{1,0:T(8,128)(2,1)} fusion(pred[]{:T(512)S(6)} %eq.12, bf16[368,512]{1,0:T(8,128)(2,1)} %copy-done.5, bf16[368,512]{1,0:T(8,128)(2,1)S(1)} %get-tuple-element.32, bf16[512,256]{1,0:T(8,128)(2,1)} %get-tuple-element.25, bf16[512,256]{1,0:T(8,128)(2,1)} %get-tuple-element.26, ...), kind=kOutput, calls=%fused_computation.8 | convolution fusion | flops 782925824 | bytes 4358145 | tf_op jit(solution)/shard_map/dot_general | solution.py:11
  140.1 1.7 fusion.2
  141.7 16.7 %collective-permute-done.4 = bf16[256,2048]{1,0:T(8,128)(2,1)} collective-permute-done((bf16[256,2048]{1,0:T(8,128)(2,1)}, bf16[256,2048]{1,0:T(8,128)(2,1)}, u32[]{:S(2)}, u32[]{:S(2)}) %collective-permute-start.4) | collective-permute-done | bytes 1048608 | tf_op jit(solution)/shard_map/ppermute | solution.py:17
  158.4 2.0 add_convert_fusion
  160.4 1.0 copy-done.2
  161.5 1.5 collective-permute-start.6
  163.1 1.4 collective-permute-start.7
  164.5 2.1 collective-permute-start.14
  166.6 3.3 %collective-permute-done.14 = f32[4,368]{1,0:T(4,128)S(1)} collective-permute-done((f32[4,368]{1,0:T(4,128)S(1)}, f32[4,368]{1,0:T(4,128)S(1)}, u32[]{:S(2)}, u32[]{:S(2)}) %collective-permute-start.14) | collective-permute-done | bytes 5920 | tf_op jit(solution)/shard_map/ppermute | solution.py:43
  169.9 1.5 collective-permute-start.15
  171.4 3.3 %collective-permute-done.7 = bf16[64,2048]{1,0:T(8,128)(2,1)S(1)} collective-permute-done((bf16[64,2048]{1,0:T(8,128)(2,1)S(1)}, bf16[64,2048]{1,0:T(8,128)(2,1)S(1)}, u32[]{:S(2)}, u32[]{:S(2)}) %collective-permute-start.7) | collective-permute-done | bytes 262176 | tf_op jit(solution)/shard_map/ppermute | solution.py:58
  174.8 1.1 constant_dynamic-update-slice_fusion.5
  176.0 1.3 collective-permute-start.8
  177.3 1.5 collective-permute-start.9
  180.1 3.7 %collective-permute-done.8 = bf16[64,2048]{1,0:T(8,128)(2,1)S(1)} collective-permute-done((bf16[64,2048]{1,0:T(8,128)(2,1)S(1)}, bf16[64,2048]{1,0:T(8,128)(2,1)S(1)}, u32[]{:S(2)}, u32[]{:S(2)}) %collective-permute-start.8) | collective-permute-done | bytes 262176 | tf_op jit(solution)/shard_map/ppermute | solution.py:64
  183.9 2.6 %collective-permute-done.9 = bf16[64,2048]{1,0:T(8,128)(2,1)S(1)} collective-permute-done((bf16[64,2048]{1,0:T(8,128)(2,1)S(1)}, bf16[64,2048]{1,0:T(8,128)(2,1)S(1)}, u32[]{:S(2)}, u32[]{:S(2)}) %collective-permute-start.9) | collective-permute-done | bytes 262176 | tf_op jit(solution)/shard_map/ppermute | solution.py:64
  186.6 1.0 broadcast_select_fusion.6
  187.6 1.5 collective-permute-start.12
  189.1 4.3 %reduce-scatter.6.cloned.1.call-done = bf16[736,256]{1,0:T(8,128)(2,1)} async-done(((bf16[736,1024]{1,0:T(8,128)(2,1)}), bf16[736,256]{1,0:T(8,128)(2,1)}) %reduce-scatter.6.cloned.1.call-update) | async-done | bytes 376848 | tf_op jit(solution)/shard_map/reduce_scatter | solution.py:144
  193.4 1.5 collective-permute-start.11
  194.9 1.4 broadcast_select_fusion.5
  196.4 0.9 maximum_convert_fusion
  197.3 31.6 %reduce-scatter.4.cloned.1.call-done = bf16[736,256]{1,0:T(8,128)(2,1)} async-done(((bf16[736,1024]{1,0:T(8,128)(2,1)}), bf16[736,256]{1,0:T(8,128)(2,1)}) %reduce-scatter.4.cloned.1.call-update) | async-done | bytes 376848 | tf_op jit(solution)/shard_map/reduce_scatter | solution.py:144
  228.9 1.1 broadcast_select_fusion.9
  230.0 0.9 convert_bitcast_fusion
  (116 shorter events, 9.3 us)
Async XLA Ops:
  7.2 71.3 %all-gather.6.cloned.1.call-start = ((), (), s32[]{:S(2)}) async-start(), calls=%async_computation.4 | async-start | bytes 1884160 | tf_op jit(solution)/shard_map/all_gather | solution.py:102
  7.2 16.9 %copy-start.6 = (bf16[256,2048]{1,0:T(8,128)(2,1)S(1)}, bf16[256,2048]{1,0:T(8,128)(2,1)}, u32[]{:S(2)}) copy-start(bf16[256,2048]{1,0:T(8,128)(2,1)} %param.11) | copy-start | bytes 3145732
  7.2 16.9 %copy-start.23 = (f32[2048]{0:T(1024)S(1)}, f32[2048]{0:T(1024)}, u32[]{:S(2)}) copy-start(f32[2048]{0:T(1024)} %param.17) | copy-start | bytes 24580
  8.8 16.0 %copy-start.8 = (f32[736,256]{1,0:T(8,128)S(1)}, f32[736,256]{1,0:T(8,128)}, u32[]{:S(2)}) copy-start(f32[736,256]{1,0:T(8,128)} %param.14) | copy-start | bytes 2260996
  9.7 17.0 %copy-start.22 = (f32[3,736]{1,0:T(4,128)S(1)}, f32[3,736]{1,0:T(4,128)}, u32[]{:S(2)}) copy-start(f32[3,736]{1,0:T(4,128)} %param.18) | copy-start | bytes 26500
  9.7 76.9 %all-gather.8.cloned.1.call-start = ((), (), s32[]{:S(2)}) async-start(), calls=%async_computation.5 | async-start | bytes 1884160 | tf_op jit(solution)/shard_map/all_gather | solution.py:102
  9.7 11.8 %collective-permute-start.1 = (bf16[2,368,256]{2,1,0:T(8,128)(2,1)S(1)}, bf16[2,368,256]{2,1,0:T(8,128)(2,1)S(1)}, u32[]{:S(2)}, u32[]{:S(2)}) collective-permute-start(bf16[2,368,256]{2,1,0:T(8,128)(2,1)S(1)} %get-tuple-element.40), channel_id=1, source_target_pairs={{0,4},{4,0},{1,5},{5,1},{2,6},{6,2},{3,7},{7,3},{8,12},{12,8},{9,1... | collective-permute-start | bytes 1130504 | tf_op jit(solution)/shard_map/ppermute | solution.py:17
  22.3 100.0 %all-gather.4.cloned.1.call-start = ((), (), s32[]{:S(2)}) async-start(), calls=%async_computation.3 | async-start | bytes 1884160 | tf_op jit(solution)/shard_map/all_gather | solution.py:102
  22.3 54.8 %collective-permute-start.2 = (bf16[256,2048]{1,0:T(8,128)(2,1)}, bf16[256,2048]{1,0:T(8,128)(2,1)}, u32[]{:S(2)}, u32[]{:S(2)}) collective-permute-start(bf16[256,2048]{1,0:T(8,128)(2,1)} %param.10), channel_id=1, source_target_pairs={{0,4},{4,0},{1,5},{5,1},{2,6},{6,2},{3,7},{7,3},{8,12},{12,8},{9,1... | collective-permute-start | bytes 3145736 | tf_op jit(solution)/shard_map/ppermute | solution.py:17
  24.4 50.0 %copy-start.3 = (bf16[256,2048]{1,0:T(8,128)(2,1)}, bf16[256,2048]{1,0:T(8,128)(2,1)S(1)}, u32[]{:S(2)}) copy-start(bf16[256,2048]{1,0:T(8,128)(2,1)S(1)} %multiply_convert_fusion) | copy-start | bytes 3145732
  24.4 3.7 %copy-start.24 = (f32[736]{0:T(1024)S(1)}, f32[736]{0:T(1024)}, u32[]{:S(2)}) copy-start(f32[736]{0:T(1024)} %param.16) | copy-start | bytes 8836
  24.4 3.7 %copy-start.25 = (f32[736]{0:T(1024)S(1)}, f32[736]{0:T(1024)}, u32[]{:S(2)}) copy-start(f32[736]{0:T(1024)} %param.15) | copy-start | bytes 8836
  24.4 3.8 %copy-start.26 = (f32[736]{0:T(1024)S(1)}, f32[736]{0:T(1024)}, u32[]{:S(2)}) copy-start(f32[736]{0:T(1024)} %param.19) | copy-start | bytes 8836
  24.4 49.9 %collective-permute-start.3 = (bf16[256,2048]{1,0:T(8,128)(2,1)S(1)}, bf16[256,2048]{1,0:T(8,128)(2,1)}, u32[]{:S(2)}, u32[]{:S(2)}) collective-permute-start(bf16[256,2048]{1,0:T(8,128)(2,1)S(1)} %multiply_convert_fusion), channel_id=1, source_target_pairs={{0,4},{4,0},{1,5},{5,1},{2,6},{6,2},{3,7},{7,3},{8,12},{12,8},{9,1... | collective-permute-start | bytes 3145736 | tf_op jit(solution)/shard_map/ppermute | solution.py:17
  24.8 48.6 %collective-permute-start = (bf16[368,256]{1,0:T(8,128)(2,1)S(1)}, bf16[368,256]{1,0:T(8,128)(2,1)S(1)}, u32[]{:S(2)}, u32[]{:S(2)}) collective-permute-start(bf16[368,256]{1,0:T(8,128)(2,1)S(1)} %broadcast_select_fusion.14), channel_id=1, source_target_pairs={{0,4},{4,0},{1,5},{5,1},{2,6},{6,2},{3,7},{7,3},{8,12},{12,8},{9,1... | collective-permute-start | bytes 565256 | tf_op jit(solution)/shard_map/ppermute | solution.py:17
  74.3 112.2 %reduce-scatter.8.cloned.1.call-start = ((), (), s32[]{:S(2)}) async-start(), calls=%async_computation.8 | async-start | bytes 1884160 | tf_op jit(solution)/shard_map/reduce_scatter | solution.py:144
  78.5 10.1 %copy-start = (bf16[512,2048]{1,0:T(8,128)(2,1)}, bf16[512,2048]{1,0:T(8,128)(2,1)S(1)}, u32[]{:S(2)}) copy-start(bf16[512,2048]{1,0:T(8,128)(2,1)S(1)} %constant_dynamic-update-slice_fusion) | copy-start | bytes 6291460
  88.7 1.6 copy-start.1
  91.3 2.1 copy-start.9
  91.3 2.1 copy-start.4
  96.8 96.6 %reduce-scatter.6.cloned.1.call-start = ((), (), s32[]{:S(2)}) async-start(), calls=%async_computation.7 | async-start | bytes 1884160 | tf_op jit(solution)/shard_map/reduce_scatter | solution.py:144
  122.2 3.2 %copy-start.10 = (f32[368,512]{1,0:T(8,128)S(1)}, f32[368,512]{1,0:T(8,128)}, u32[]{:S(2)}) copy-start(f32[368,512]{1,0:T(8,128)} %copy-done.9) | copy-start | bytes 2260996
  122.2 3.2 %copy-start.11 = (f32[368,512]{1,0:T(8,128)S(1)}, f32[368,512]{1,0:T(8,128)}, u32[]{:S(2)}) copy-start(f32[368,512]{1,0:T(8,128)} %get-tuple-element.21) | copy-start | bytes 2260996
  122.2 3.2 %copy-start.12 = (f32[368,512]{1,0:T(8,128)S(1)}, f32[368,512]{1,0:T(8,128)}, u32[]{:S(2)}) copy-start(f32[368,512]{1,0:T(8,128)} %get-tuple-element.48) | copy-start | bytes 2260996
  125.5 2.8 %copy-start.14 = (bf16[512,256]{1,0:T(8,128)(2,1)S(1)}, bf16[512,256]{1,0:T(8,128)(2,1)}, u32[]{:S(2)}) copy-start(bf16[512,256]{1,0:T(8,128)(2,1)} %get-tuple-element.24) | copy-start | bytes 786436
  125.5 2.8 %copy-start.15 = (bf16[512,256]{1,0:T(8,128)(2,1)S(1)}, bf16[512,256]{1,0:T(8,128)(2,1)}, u32[]{:S(2)}) copy-start(bf16[512,256]{1,0:T(8,128)(2,1)} %get-tuple-element.25) | copy-start | bytes 786436
  125.5 2.8 %copy-start.16 = (bf16[512,256]{1,0:T(8,128)(2,1)S(1)}, bf16[512,256]{1,0:T(8,128)(2,1)}, u32[]{:S(2)}) copy-start(bf16[512,256]{1,0:T(8,128)(2,1)} %get-tuple-element.26) | copy-start | bytes 786436
  125.5 2.7 %copy-start.17 = (bf16[512,256]{1,0:T(8,128)(2,1)S(1)}, bf16[512,256]{1,0:T(8,128)(2,1)}, u32[]{:S(2)}) copy-start(bf16[512,256]{1,0:T(8,128)(2,1)} %get-tuple-element.27) | copy-start | bytes 786436
  125.5 2.7 %copy-start.18 = (bf16[512,256]{1,0:T(8,128)(2,1)S(1)}, bf16[512,256]{1,0:T(8,128)(2,1)}, u32[]{:S(2)}) copy-start(bf16[512,256]{1,0:T(8,128)(2,1)} %get-tuple-element.28) | copy-start | bytes 786436
  125.5 2.7 %copy-start.19 = (bf16[512,256]{1,0:T(8,128)(2,1)S(1)}, bf16[512,256]{1,0:T(8,128)(2,1)}, u32[]{:S(2)}) copy-start(bf16[512,256]{1,0:T(8,128)(2,1)} %get-tuple-element.29) | copy-start | bytes 786436
  125.5 2.7 %copy-start.20 = (bf16[512,256]{1,0:T(8,128)(2,1)S(1)}, bf16[512,256]{1,0:T(8,128)(2,1)}, u32[]{:S(2)}) copy-start(bf16[512,256]{1,0:T(8,128)(2,1)} %get-tuple-element.30) | copy-start | bytes 786436
  125.5 2.7 %copy-start.21 = (bf16[512,256]{1,0:T(8,128)(2,1)S(1)}, bf16[512,256]{1,0:T(8,128)(2,1)}, u32[]{:S(2)}) copy-start(bf16[512,256]{1,0:T(8,128)(2,1)} %get-tuple-element.31) | copy-start | bytes 786436
  127.5 0.7 copy-start.5
  130.5 98.4 %reduce-scatter.4.cloned.1.call-start = ((), (), s32[]{:S(2)}) async-start(), calls=%async_computation.6 | async-start | bytes 1884160 | tf_op jit(solution)/shard_map/reduce_scatter | solution.py:144
  134.1 24.4 %collective-permute-start.4 = (bf16[256,2048]{1,0:T(8,128)(2,1)}, bf16[256,2048]{1,0:T(8,128)(2,1)}, u32[]{:S(2)}, u32[]{:S(2)}) collective-permute-start(bf16[256,2048]{1,0:T(8,128)(2,1)} %fusion), channel_id=1, source_target_pairs={{0,4},{4,0},{1,5},{5,1},{2,6},{6,2},{3,7},{7,3},{8,12},{12,8},{9,1... | collective-permute-start | bytes 3145736 | tf_op jit(solution)/shard_map/ppermute | solution.py:17
  135.6 28.9 %collective-permute-start.13 = (f32[4,368]{1,0:T(4,128)S(1)}, f32[4,368]{1,0:T(4,128)S(1)}, u32[]{:S(2)}, u32[]{:S(2)}) collective-permute-start(f32[4,368]{1,0:T(4,128)S(1)} %pad_maximum_fusion.12), channel_id=1, source_target_pairs={{0,8},{8,0},{16,24},{24,16},{1,9},{9,1},{17,25},{25,17},{2,10},{10... | collective-permute-start | bytes 17672 | tf_op jit(solution)/shard_map/ppermute | solution.py:43
  160.4 1.0 copy-start.2
  161.5 10.0 %collective-permute-start.5 = (bf16[64,2048]{1,0:T(8,128)(2,1)S(1)}, bf16[64,2048]{1,0:T(8,128)(2,1)S(1)}, u32[]{:S(2)}, u32[]{:S(2)}) collective-permute-start(bf16[64,2048]{1,0:T(8,128)(2,1)S(1)} %get-tuple-element.33), channel_id=1, source_target_pairs={{0,1},{1,2},{2,3},{3,0},{4,5},{5,6},{6,7},{7,4},{8,9},{9,10},{10,1... | collective-permute-start | bytes 786440 | tf_op jit(solution)/shard_map/ppermute | solution.py:58
  161.5 9.9 %collective-permute-start.6 = (bf16[64,2048]{1,0:T(8,128)(2,1)S(1)}, bf16[64,2048]{1,0:T(8,128)(2,1)S(1)}, u32[]{:S(2)}, u32[]{:S(2)}) collective-permute-start(bf16[64,2048]{1,0:T(8,128)(2,1)S(1)} %get-tuple-element.35), channel_id=1, source_target_pairs={{0,2},{1,3},{2,0},{3,1},{4,6},{5,7},{6,4},{7,5},{8,10},{9,11},{10,... | collective-permute-start | bytes 786440 | tf_op jit(solution)/shard_map/ppermute | solution.py:58
  163.1 11.7 %collective-permute-start.7 = (bf16[64,2048]{1,0:T(8,128)(2,1)S(1)}, bf16[64,2048]{1,0:T(8,128)(2,1)S(1)}, u32[]{:S(2)}, u32[]{:S(2)}) collective-permute-start(bf16[64,2048]{1,0:T(8,128)(2,1)S(1)} %get-tuple-element.34), channel_id=1, source_target_pairs={{0,3},{1,0},{2,1},{3,2},{4,7},{5,4},{6,5},{7,6},{8,11},{9,8},{10,9... | collective-permute-start | bytes 786440 | tf_op jit(solution)/shard_map/ppermute | solution.py:58
  164.5 5.4 %collective-permute-start.14 = (f32[4,368]{1,0:T(4,128)S(1)}, f32[4,368]{1,0:T(4,128)S(1)}, u32[]{:S(2)}, u32[]{:S(2)}) collective-permute-start(f32[4,368]{1,0:T(4,128)S(1)} %fusion.38), channel_id=1, source_target_pairs={{0,16},{8,24},{16,0},{24,8},{1,17},{9,25},{17,1},{25,9},{2,18},{10... | collective-permute-start | bytes 17672 | tf_op jit(solution)/shard_map/ppermute | solution.py:43
  169.9 7.3 %collective-permute-start.15 = (f32[4,368]{1,0:T(4,128)S(1)}, f32[4,368]{1,0:T(4,128)S(1)}, u32[]{:S(2)}, u32[]{:S(2)}) collective-permute-start(f32[4,368]{1,0:T(4,128)S(1)} %fusion.47), channel_id=1, source_target_pairs={{0,4},{4,0},{1,5},{5,1},{2,6},{6,2},{3,7},{7,3},{8,12},{12,8},{9,1... | collective-permute-start | bytes 17672 | tf_op jit(solution)/shard_map/ppermute | solution.py:17
  176.0 7.9 %collective-permute-start.8 = (bf16[64,2048]{1,0:T(8,128)(2,1)S(1)}, bf16[64,2048]{1,0:T(8,128)(2,1)S(1)}, u32[]{:S(2)}, u32[]{:S(2)}) collective-permute-start(bf16[64,2048]{1,0:T(8,128)(2,1)S(1)} %get-tuple-element.19), channel_id=1, source_target_pairs={{0,1},{1,2},{2,3},{3,0},{4,5},{5,6},{6,7},{7,4},{8,9},{9,10},{10,1... | collective-permute-start | bytes 786440 | tf_op jit(solution)/shard_map/ppermute | solution.py:64
  177.3 9.2 %collective-permute-start.9 = (bf16[64,2048]{1,0:T(8,128)(2,1)S(1)}, bf16[64,2048]{1,0:T(8,128)(2,1)S(1)}, u32[]{:S(2)}, u32[]{:S(2)}) collective-permute-start(bf16[64,2048]{1,0:T(8,128)(2,1)S(1)} %get-tuple-element.19), channel_id=1, source_target_pairs={{0,2},{1,3},{2,0},{3,1},{4,6},{5,7},{6,4},{7,5},{8,10},{9,11},{10,... | collective-permute-start | bytes 786440 | tf_op jit(solution)/shard_map/ppermute | solution.py:64
  180.1 14.7 %collective-permute-start.10 = (bf16[64,2048]{1,0:T(8,128)(2,1)S(1)}, bf16[64,2048]{1,0:T(8,128)(2,1)S(1)}, u32[]{:S(2)}, u32[]{:S(2)}) collective-permute-start(bf16[64,2048]{1,0:T(8,128)(2,1)S(1)} %get-tuple-element.19), channel_id=1, source_target_pairs={{0,3},{1,0},{2,1},{3,2},{4,7},{5,4},{6,5},{7,6},{8,11},{9,8},{10,9... | collective-permute-start | bytes 786440 | tf_op jit(solution)/shard_map/ppermute | solution.py:64
  187.6 7.3 %collective-permute-start.12 = (bf16[368,256]{1,0:T(8,128)(2,1)S(1)}, bf16[368,256]{1,0:T(8,128)(2,1)S(1)}, u32[]{:S(2)}, u32[]{:S(2)}) collective-permute-start(bf16[368,256]{1,0:T(8,128)(2,1)S(1)} %broadcast_select_fusion.6), channel_id=1, source_target_pairs={{0,4},{4,0},{1,5},{5,1},{2,6},{6,2},{3,7},{7,3},{8,12},{12,8},{9,1... | collective-permute-start | bytes 565256 | tf_op jit(solution)/shard_map/ppermute | solution.py:17
  193.4 35.5 %collective-permute-start.11 = (bf16[736,256]{1,0:T(8,128)(2,1)}, bf16[736,256]{1,0:T(8,128)(2,1)S(1)}, u32[]{:S(2)}, u32[]{:S(2)}) collective-permute-start(bf16[736,256]{1,0:T(8,128)(2,1)} %reduce-scatter.6.cloned.1.call-done), channel_id=1, source_target_pairs={{0,4},{4,0},{1,5},{5,1},{2,6},{6,2},{3,7},{7,3},{8,12},{12,8},{9,1... | collective-permute-start | bytes 1130504 | tf_op jit(solution)/shard_map/ppermute | solution.py:17
  194.9 36.0 %copy-start.7 = (bf16[256,2048]{1,0:T(8,128)(2,1)}, bf16[256,2048]{1,0:T(8,128)(2,1)S(1)}, u32[]{:S(2)}) copy-start(bf16[256,2048]{1,0:T(8,128)(2,1)S(1)} %constant_dynamic-update-slice_fusion.2) | copy-start | bytes 3145732
  (1 other events, 0.7 us)
Sparse Core Ops, SparseCore 0:
  10.1 39.3 all-gather.5
  51.7 34.8 all-gather.7
  88.1 34.0 all-gather.3
  124.4 33.4 reduce-scatter.7
  160.1 33.2 reduce-scatter.5
  195.6 33.2 reduce-scatter.3
